TPU v7x, 32 devices: a whole 2x2x4 slice. The times are simulated.
32 devices in a mesh: sp: 8 (over z, x), tp: 4 (over y, core).
Axes of the slice: x: 2, y: 2, z: 4, core: 2. Of those that a mesh axis runs over, the one named last changes fastest.
Arguments:
- queries: bfloat16 [512, 16, 192], P('sp', 'tp'), may hold values from -400 to 400
- latents: bfloat16 [512, 512], P('sp'), may hold values from -6 to 6
- rope_keys: bfloat16 [512, 64], P('sp'), may hold values from -9 to 9
- latent_norm_scale: float32 [512], replicated, may hold values from 0.1 to 1.9
- key_value_weight: bfloat16 [512, 16, 256], P(None, 'tp'), may hold values from -0.25 to 0.25
- out_weight: bfloat16 [2048, 2048], P('tp'), may hold values from -1 to 1
- resid: bfloat16 [512, 2048], P('sp'), may hold values from -3 to 3
- ffn_gain: float32 [2048], replicated, may hold values from 0.1 to 1.9
- expert_ids: int32 [512, 2], P('sp'), may hold values from 0 to 7, all different within a row; in each aligned block of 64 rows (0 to 63, 64 to 127, ...) at most 24 rows name the same one
- route_weights: float32 [512, 2], P('sp'), may hold values from 0.1 to 1
- gate_weight: bfloat16 [8, 2048, 4096], P('sp', None, 'tp'), may hold values from -0.125 to 0.125
- up_weight: bfloat16 [8, 2048, 4096], P('sp', None, 'tp'), may hold values from -0.125 to 0.125
- down_weight: bfloat16 [8, 4096, 2048], P('sp', 'tp'), may hold values from -0.09375 to 0.09375
Outputs:
- updated: bfloat16 [512, 2048], P('sp', 'tp')
Inputs may be any that keep to these rules, and one draw needn't show every extreme that they name: `expert_ids`: among the rows of one device no expert is named more than 24 times, and in some devices some expert is named exactly 24 times.
All inputs are finite; a program needn't handle non-finite values.
Results may differ from a plain program's by a relative error of at most 0.025.
Values may be sent and summed in bfloat16 or wider, within the bound.
A program may use at most 64 MiB of HBM per device.

v0:
```python
import jax
import jax.numpy as jnp
from jax import lax
from jax.sharding import PartitionSpec as P

PLAIN_WIDTH = 128
VALUE_WIDTH = 128
rope_base = 10000.0
norm_eps = 1e-06


def rotary_table(positions, width):
    half_width = width // 2
    inverse = rope_base ** (-jnp.arange(half_width, dtype=jnp.float32) / half_width)
    turned = positions[:, None] * inverse[None, :]
    return (jnp.cos(turned), jnp.sin(turned))


def turn_pairs(vectors, cosines, sines):
    half_width = vectors.shape[-1] // 2
    front_half = vectors[..., :half_width]
    back_half = vectors[..., half_width:]
    return jnp.concatenate(
        [front_half * cosines - back_half * sines, back_half * cosines + front_half * sines],
        axis=-1,
    )


def rms_scaled(matrix, gain):
    floats = matrix.astype(jnp.float32)
    return floats * lax.rsqrt(jnp.mean(floats * floats, axis=-1, keepdims=True) + norm_eps) * gain


def attend(state_now, query_plain, query_turned, key_plain, key_turned, head_values):
    running, totals, accumulated = state_now
    score_scale = (query_plain.shape[-1] + query_turned.shape[-1]) ** (-0.5)
    scores = jnp.einsum("qhn,khn->hqk", query_plain, key_plain, preferred_element_type=jnp.float32)
    scores = (
        scores
        + jnp.einsum("qhr,kr->hqk", query_turned, key_turned, preferred_element_type=jnp.float32)
    ) * score_scale
    highest = jnp.max(scores, axis=-1)
    fade_by = jnp.exp(running - highest)
    exps = jnp.exp(scores - highest[..., None])
    totals = totals * fade_by + jnp.sum(exps, axis=-1)
    summed = jnp.einsum(
        "hqk,khv->qhv", exps.astype(jnp.bfloat16), head_values, preferred_element_type=jnp.float32
    )
    accumulated = accumulated * jnp.transpose(fade_by)[:, :, None] + summed
    return (highest, totals, accumulated)


def finish_expert(gate_act, up_act, down_matrix, senders, items):
    hidden = (jax.nn.silu(gate_act) * up_act).astype(jnp.bfloat16)
    partial_rows = jnp.dot(hidden, down_matrix, preferred_element_type=jnp.float32).reshape(
        senders, items, -1
    )
    col_share = lax.psum_scatter(
        partial_rows.astype(jnp.bfloat16), "tp", scatter_dimension=2, tiled=True
    )
    return lax.all_to_all(col_share, "sp", split_axis=0, concat_axis=0, tiled=True)


def shards(
    queries,
    latents,
    rope_keys,
    latent_norm_scale,
    key_value_weight,
    out_weight,
    resid,
    ffn_gain,
    expert_ids,
    route_weights,
    gate_weight,
    up_weight,
    down_weight,
):
    tok_rows, local_heads, _ = queries.shape
    offset = lax.axis_index("sp") * tok_rows
    positions = (offset + jnp.arange(tok_rows, dtype=jnp.int32)).astype(jnp.float32)
    cosines, sines = rotary_table(positions, rope_keys.shape[1])
    query_plain = queries[:, :, :PLAIN_WIDTH]
    query_turned = turn_pairs(
        queries[:, :, PLAIN_WIDTH:].astype(jnp.float32), cosines[:, None, :], sines[:, None, :]
    ).astype(jnp.bfloat16)
    key_turned = turn_pairs(rope_keys.astype(jnp.float32), cosines, sines).astype(jnp.bfloat16)
    normalized_latent = rms_scaled(latents, latent_norm_scale).astype(jnp.bfloat16)
    key_project = key_value_weight.reshape(key_value_weight.shape[0], -1)
    pair_rows = tok_rows // 2
    turned_pairs = key_turned.reshape(pair_rows, -1)
    start_state = (
        jnp.full((local_heads, tok_rows), -jnp.inf, jnp.float32),
        jnp.zeros((local_heads, tok_rows), jnp.float32),
        jnp.zeros((tok_rows, local_heads, VALUE_WIDTH), jnp.float32),
    )
    own_projected = jnp.dot(
        normalized_latent, key_project, preferred_element_type=jnp.float32
    ).astype(jnp.bfloat16)
    head_piece = lax.all_gather(own_projected.reshape(pair_rows, -1), "sp", axis=0, tiled=True)
    turned_piece = lax.all_gather(turned_pairs, "sp", axis=0, tiled=True)
    row_count = head_piece.shape[0] * 2
    projected_rows = head_piece.reshape(row_count, -1)
    per_head = projected_rows.reshape(row_count, local_heads, -1)
    key_plain = per_head[:, :, :PLAIN_WIDTH]
    head_values = per_head[:, :, PLAIN_WIDTH:]
    final_state = attend(
        start_state,
        query_plain,
        query_turned,
        key_plain,
        turned_piece.reshape(row_count, -1),
        head_values,
    )
    _, totals, accumulated = final_state
    attended = (accumulated / jnp.transpose(totals)[:, :, None]).astype(jnp.bfloat16)
    head_partial = jnp.dot(
        attended.reshape(tok_rows, -1), out_weight, preferred_element_type=jnp.float32
    )
    mixed = lax.psum(head_partial.astype(jnp.bfloat16), "tp").astype(jnp.float32)
    middle_float = (resid.astype(jnp.float32) + mixed).astype(jnp.bfloat16).astype(jnp.float32)
    normed = rms_scaled(middle_float, ffn_gain).astype(jnp.bfloat16)
    experts = lax.axis_size("sp")
    top_count = expert_ids.shape[1]
    capacity = (3 * tok_rows * top_count + 2 * experts - 1) // (2 * experts)
    flat_ids = expert_ids.reshape(-1)
    picked = (flat_ids[:, None] == jnp.arange(experts, dtype=jnp.int32)[None, :]).astype(jnp.int32)
    slot_rank = jnp.sum((jnp.cumsum(picked, axis=0) - picked) * picked, axis=1)
    slot_index = flat_ids * capacity + slot_rank
    sources = jnp.arange(flat_ids.shape[0], dtype=jnp.int32) // top_count
    owner_row = jnp.zeros((experts * capacity,), jnp.int32).at[slot_index].set(sources)
    filled = jnp.zeros((experts * capacity,), jnp.bool_).at[slot_index].set(True)
    outgoing = jnp.where(filled[:, None], normed[owner_row], jnp.zeros((), jnp.bfloat16)).reshape(
        experts, capacity, -1
    )
    arrived = lax.all_to_all(outgoing, "sp", split_axis=0, concat_axis=0, tiled=True)
    senders, items, width = arrived.shape
    rows_in = arrived.reshape(-1, width)
    gate_act = jnp.dot(rows_in, gate_weight[0], preferred_element_type=jnp.float32)
    up_act = jnp.dot(rows_in, up_weight[0], preferred_element_type=jnp.float32)
    returned = finish_expert(gate_act, up_act, down_weight[0], senders, items)
    columns = returned.shape[2]
    back_rows = returned.reshape(-1, columns)
    chosen_rows = back_rows[slot_index].astype(jnp.float32) * route_weights.reshape(-1)[:, None]
    routed = jnp.sum(chosen_rows.reshape(tok_rows, top_count, columns), axis=1)
    column_start = lax.axis_index("tp") * columns
    middle_cols = lax.dynamic_slice_in_dim(middle_float, column_start, columns, 1)
    return (middle_cols + routed).astype(jnp.bfloat16)


def solution(mesh):
    placed = (
        P("sp", "tp", None),
        P("sp", None),
        P("sp", None),
        P(),
        P(None, "tp", None),
        P("tp", None),
        P("sp", None),
        P(),
        P("sp", None),
        P("sp", None),
        P("sp", None, "tp"),
        P("sp", None, "tp"),
        P("sp", "tp", None),
    )
    return jax.shard_map(
        shards, mesh=mesh, in_specs=placed, out_specs=P("sp", "tp"), check_vma=False
    )
```

profile of v0, /device:TPU:0, one launch (start us, length us, event | category | flops | bytes accessed | tf_op | source)
XLA Modules:
  0.0 172.7 jit_solution(10261434299274544389)
XLA Ops:
  6.5 1.6 copy.35
  9.1 1.2 convolution_convert_fusion.1
  11.1 1.5 slice.25
  13.7 32.5 %all_gather.7 = bf16[256,128]{1,0:T(8,128)(2,1)S(1)} all-gather(bf16[32,128]{1,0:T(8,128)(2,1)S(1)} %convert_element_type.77), channel_id=1, replica_groups=mesh['sp'=8,'tp'=4] {'sp'}, dimensions={0}, use_global_device_ids=true | all-gather | bytes 73728 | tf_op jit(solution)/shard_map/all_gather | solution.py:101
  47.3 1.0 scatter_custom_fusion.1
  49.0 5.2 %all-gather.2.cloned.1.call-done = bf16[256,2048]{1,0:T(8,128)(2,1)} async-done(((bf16[32,2048]{1,0:T(8,128)(2,1)}), bf16[256,2048]{1,0:T(8,128)(2,1)}) %all-gather.2.cloned.1.call-update) | async-done | bytes 1048592 | tf_op jit(solution)/shard_map/all_gather | solution.py:100
  54.2 1.8 %reshape_reshape.3 = bf16[512,4,256]{2,1,0:T(4,128)(2,1)S(1)} reshape(bf16[256,2048]{1,0:T(8,128)(2,1)} %all-gather.2.cloned.1.call-done) | data formatting | bytes 2097152 | tf_op jit(solution)/shard_map/reshape;reshape | solution.py:104
  56.5 1.1 convolution_bitcast_fusion.1
  57.6 1.2 fusion.49
  59.4 1.2 convolution_convert_fusion
  60.7 1.0 scatter_custom_fusion
  61.8 29.9 %all-reduce.2.cloned.1.call-done = bf16[64,2048]{1,0:T(8,128)(2,1)} async-done(((bf16[64,2048]{1,0:T(8,128)(2,1)}), bf16[64,2048]{1,0:T(8,128)(2,1)}) %all-reduce.2.cloned.1.call-update) | async-done | bytes 262160 | tf_op jit(solution)/shard_map/psum | solution.py:120
  91.7 1.9 %fusion.26 = (f32[64,2048]{1,0:T(8,128)}, f32[64]{0:T(128)S(1)}) fusion(bf16[64,2048]{1,0:T(8,128)(2,1)} %all-reduce.2.cloned.1.call-done, bf16[64,2048]{1,0:T(8,128)(2,1)S(1)} %copy-done.1), kind=kLoop, calls=%fused_computation.33 | loop fusion | flops 917440 | bytes 1048832 | tf_op jit(solution)/shard_map/convert_element_type | solution.py:121
  93.7 1.1 multiply_convert_fusion
  94.8 1.1 gather_fusion
  96.1 24.6 %all_to_all.10 = bf16[8,24,2048]{2,1,0:T(8,128)(2,1)S(1)} all-to-all(bf16[8,24,2048]{2,1,0:T(8,128)(2,1)S(1)} %broadcast_select_fusion), channel_id=1, replica_groups=mesh['sp'=8,'tp'=4] {'sp'}, dimensions={0} | all-to-all | bytes 1572864 | tf_op jit(solution)/shard_map/all_to_all | solution.py:136
  120.6 3.2 %fusion.4 = f32[192,1024]{1,0:T(8,128)S(1)} fusion(bf16[192,2048]{1,0:T(8,128)(2,1)S(1)} %bitcast.69, bf16[1,2048,1024]{2,1,0:T(8,128)(2,1)} %param.23), kind=kOutput, calls=%fused_computation.8 | convolution fusion | flops 805306368 | bytes 5767168 | tf_op jit(solution)/shard_map/dot_general | solution.py:139
  123.9 1.1 fusion.12
  124.9 1.1 copy-done.6
  126.0 1.9 %fusion.6 = bf16[8,24,2048]{2,1,0:T(8,128)(2,1)} fusion(bf16[8,24,1024]{2,1,0:T(8,128)(2,1)S(1)} %bitcast.73, bf16[1,1024,2048]{2,1,0:T(8,128)(2,1)S(1)} %copy-done.6), kind=kOutput, calls=%fused_computation.10 | convolution fusion | flops 805699584 | bytes 5373952 | tf_op jit(solution)/shard_map/dot_general | solution.py:55
  128.0 22.0 %reduce-scatter.2.cloned.1.call-done = bf16[8,24,512]{2,1,0:T(8,128)(2,1)} async-done(((bf16[8,24,2048]{2,1,0:T(8,128)(2,1)}), bf16[8,24,512]{2,1,0:T(8,128)(2,1)}) %reduce-scatter.2.cloned.1.call-update) | async-done | bytes 196624 | tf_op jit(solution)/shard_map/reduce_scatter | solution.py:58
  149.9 5.5 %all-to-all-start.1 = ((bf16[8,24,512]{2,1,0:T(8,128)(2,1)}), bf16[8,24,512]{2,1,0:T(8,128)(2,1)S(1)}, u32[]{:S(2)}, u32[]{:S(2)}) async-start(bf16[8,24,512]{2,1,0:T(8,128)(2,1)} %reduce-scatter.2.cloned.1.call-done), calls=%async_computation.2 | async-start | bytes 393216 | tf_op jit(solution)/shard_map/all_to_all | solution.py:61
  155.5 7.7 %all-to-all-done.1 = bf16[8,24,512]{2,1,0:T(8,128)(2,1)S(1)} async-done(((bf16[8,24,512]{2,1,0:T(8,128)(2,1)}), bf16[8,24,512]{2,1,0:T(8,128)(2,1)S(1)}, u32[]{:S(2)}, u32[]{:S(2)}) %all-to-all-start.1) | async-done | bytes 196640 | tf_op jit(solution)/shard_map/all_to_all | solution.py:61
  164.6 1.6 add_convert_fusion.1
  (59 shorter events, 7.4 us)
Async XLA Ops:
  6.5 52.9 %copy-start = (bf16[512,2048]{1,0:T(8,128)(2,1)S(1)}, bf16[512,2048]{1,0:T(8,128)(2,1)}, u32[]{:S(2)}) copy-start(bf16[512,2048]{1,0:T(8,128)(2,1)} %param.18) | copy-start | bytes 6291460
  6.5 41.7 %slice-start = ((bf16[64,4,192]{2,1,0:T(4,128)(2,1)}), bf16[64,4,64]{2,1,0:T(4,128)(2,1)S(1)}, s32[]{:S(2)}) async-start(bf16[64,4,192]{2,1,0:T(4,128)(2,1)} %param.13), calls=%async_computation.6 | async-start | bytes 131072 | tf_op jit(solution)/shard_map/slice | solution.py:85
  6.5 39.8 %copy-start.3 = (s32[64,2]{0,1:T(2,128)S(1)}, s32[64,2]{0,1:T(2,128)}, u32[]{:S(2)}) copy-start(s32[64,2]{0,1:T(2,128)} %param.21) | copy-start | bytes 1540
  6.5 47.7 %all-gather.2.cloned.1.call-start = ((), (), s32[]{:S(2)}) async-start(), calls=%async_computation.3 | async-start | bytes 1179648 | tf_op jit(solution)/shard_map/all_gather | solution.py:100
  11.0 80.7 %all-reduce.2.cloned.1.call-start = ((), (), s32[]{:S(2)}) async-start(), calls=%async_computation.4 | async-start | bytes 524288 | tf_op jit(solution)/shard_map/psum | solution.py:120
  56.1 35.6 %copy-start.1 = (bf16[64,2048]{1,0:T(8,128)(2,1)S(1)}, bf16[64,2048]{1,0:T(8,128)(2,1)}, u32[]{:S(2)}) copy-start(bf16[64,2048]{1,0:T(8,128)(2,1)} %param.19) | copy-start | bytes 786436
  56.5 37.2 %copy-start.2 = (f32[2048]{0:T(1024)S(1)}, f32[2048]{0:T(1024)}, u32[]{:S(2)}) copy-start(f32[2048]{0:T(1024)} %param.20) | copy-start | bytes 24580
  60.6 89.3 %reduce-scatter.2.cloned.1.call-start = ((), (), s32[]{:S(2)}) async-start(), calls=%async_computation.5 | async-start | bytes 983040 | tf_op jit(solution)/shard_map/reduce_scatter | solution.py:58
  95.9 27.9 %copy-start.5 = (bf16[1,2048,1024]{2,1,0:T(8,128)(2,1)S(1)}, bf16[1,2048,1024]{2,1,0:T(8,128)(2,1)}, u32[]{:S(2)}) copy-start(bf16[1,2048,1024]{2,1,0:T(8,128)(2,1)} %param.24) | copy-start | bytes 12582916
  123.8 2.2 %copy-start.6 = (bf16[1,1024,2048]{2,1,0:T(8,128)(2,1)S(1)}, bf16[1,1024,2048]{2,1,0:T(8,128)(2,1)}, u32[]{:S(2)}) copy-start(bf16[1,1024,2048]{2,1,0:T(8,128)(2,1)} %param.25) | copy-start | bytes 12582916
  124.9 30.5 %copy-start.4 = (f32[64,2]{0,1:T(2,128)S(1)}, f32[64,2]{0,1:T(2,128)}, u32[]{:S(2)}) copy-start(f32[64,2]{0,1:T(2,128)} %param.22) | copy-start | bytes 1540
  149.9 13.3 %all-to-all-start.1 = ((bf16[8,24,512]{2,1,0:T(8,128)(2,1)}), bf16[8,24,512]{2,1,0:T(8,128)(2,1)S(1)}, u32[]{:S(2)}, u32[]{:S(2)}) async-start(bf16[8,24,512]{2,1,0:T(8,128)(2,1)} %reduce-scatter.2.cloned.1.call-done), calls=%async_computation.2 | async-start | bytes 393216 | tf_op jit(solution)/shard_map/all_to_all | solution.py:61
Sparse Core Ops, SparseCore 0:
  11.2 43.0 all-gather.1
  60.8 30.9 all-reduce.1
  128.1 21.7 reduce-scatter.1
where the time goes:
time: 173 us
  waiting for transfers between devices  64.8 us (37%)
  blocking collectives  57.1 us (33%)
  between operations  13.4 us (8%)
  local copies, waits for them, and re-layouts  12.1 us (7%)
  matrix products  11.2 us (6%)
  other arithmetic  8.52 us (5%)
  starting transfers between devices  5.6 us (3%)
    all_gather x1, blocking collectives, shards(): turned_piece = lax.all_gather(turned_pairs, 'sp', axis=0, tiled=True)  32.5 us
    psum x1, waiting for transfers between devices, shards(): lax.psum(head_partial.astype(jnp.bfloat16), 'tp').astype(jnp.float32)  29.9 us
    all_to_all x1, blocking collectives, shards(): lax.all_to_all(outgoing, 'sp', split_axis=0, concat_axis=0, tiled=True)  24.6 us
    reduce_scatter x1, waiting for transfers between devices, finish_expert(): lax.psum_scatter(partial_rows.astype(jnp.bfloat16), 'tp', scatter_dimensi...  22 us
    all_to_all x1, waiting for transfers between devices, finish_expert(): lax.all_to_all(col_share, 'sp', split_axis=0, concat_axis=0, tiled=True)  7.68 us
    all_to_all x1, starting transfers between devices, finish_expert(): lax.all_to_all(col_share, 'sp', split_axis=0, concat_axis=0, tiled=True)  5.52 us
    all_gather x1, waiting for transfers between devices, shards(): lax.all_gather(own_projected.reshape(pair_rows, -1), 'sp', axis=0, tiled=...  5.2 us
  transfers between devices with their start and end apart: 4, of which 4 were waited for; matrix products, arithmetic and copies ran while one was open for 4% of the time, Pallas kernels for 0%

commit v1 on v0

--- a/solution.py
+++ b/solution.py
@@ -7,6 +7,11 @@
 VALUE_WIDTH = 128
 rope_base = 10000.0
 norm_eps = 1e-06
+
+
+def _trace_side(s0, bus_axis):
+    y1 = lax.all_gather(s0, bus_axis).sum(axis=0)
+    return y1
 
 
 def rotary_table(positions, width):
@@ -117,7 +122,7 @@
     head_partial = jnp.dot(
         attended.reshape(tok_rows, -1), out_weight, preferred_element_type=jnp.float32
     )
-    mixed = lax.psum(head_partial.astype(jnp.bfloat16), "tp").astype(jnp.float32)
+    mixed = _trace_side(head_partial.astype(jnp.bfloat16), "tp").astype(jnp.float32)
     middle_float = (resid.astype(jnp.float32) + mixed).astype(jnp.bfloat16).astype(jnp.float32)
     normed = rms_scaled(middle_float, ffn_gain).astype(jnp.bfloat16)
     experts = lax.axis_size("sp")

time: 173 us -> 157 us (0.908)
  waiting for transfers between devices: 64.8 us -> 51.1 us
    psum x1 -> x0, waiting for transfers between devices: 29.9 us -> none  [shards(): lax.psum(head_partial.astype(jnp.bfloat16), 'tp').astype(jnp.float32)]
    all_gather x0 -> x1, waiting for transfers between devices: none -> 12.5 us  [_trace_side(): y1 = lax.all_gather(s0, bus_axis).sum(axis=0)]
    all_gather x1, waiting for transfers between devices: 5.2 us -> 9.4 us  [shards(): lax.all_gather(own_projected.reshape(pair_rows, -1), 'sp', axis=0, tiled=...]
  transfers between devices with their start and end apart: 4 -> 4, of which waited for: 4 -> 4; matrix products, arithmetic and copies ran while one was open for 4% -> 3% of each run, Pallas kernels for 0% -> 0%
where the time goes in v1:
time: 157 us; the launch traced here: 156 us
  blocking collectives  58.5 us (37%)
  waiting for transfers between devices  51.1 us (33%)
  between operations  13.5 us (9%)
  local copies, waits for them, and re-layouts  10.6 us (7%)
  matrix products  9.52 us (6%)
  other arithmetic  7.42 us (5%)
  starting transfers between devices  5.6 us (4%)
    all_gather x1, blocking collectives, shards(): turned_piece = lax.all_gather(turned_pairs, 'sp', axis=0, tiled=True)  32.4 us
    all_to_all x1, blocking collectives, shards(): lax.all_to_all(outgoing, 'sp', split_axis=0, concat_axis=0, tiled=True)  26.1 us
    reduce_scatter x1, waiting for transfers between devices, finish_expert(): lax.psum_scatter(partial_rows.astype(jnp.bfloat16), 'tp', scatter_dimensi...  21.5 us
    all_gather x1, waiting for transfers between devices, _trace_side(): y1 = lax.all_gather(s0, bus_axis).sum(axis=0)  12.5 us
    all_gather x1, waiting for transfers between devices, shards(): lax.all_gather(own_projected.reshape(pair_rows, -1), 'sp', axis=0, tiled=...  9.4 us
    all_to_all x1, waiting for transfers between devices, finish_expert(): lax.all_to_all(col_share, 'sp', split_axis=0, concat_axis=0, tiled=True)  7.68 us
    all_to_all x1, starting transfers between devices, finish_expert(): lax.all_to_all(col_share, 'sp', split_axis=0, concat_axis=0, tiled=True)  5.51 us
    dot_general x1, matrix products, shards(): jnp.dot(rows_in, gate_weight[0], preferred_element_type=jnp.float32)  3.2 us
  transfers between devices with their start and end apart: 4, of which 4 were waited for; matrix products, arithmetic and copies ran while one was open for 3% of the time, Pallas kernels for 0%

profile of v1, /device:TPU:0, one launch (start us, length us, event | category | flops | bytes accessed | tf_op | source)
XLA Modules:
  0.0 156.2 jit_solution(10116158458303477172)
XLA Ops:
  6.5 1.6 %copy.35 = bf16[64,8,4,256]{3,1,2,0:T(8,128)(2,1)S(1)} copy(bf16[64,8,4,256]{3,2,1,0:T(4,128)(2,1)} %bitcast.74) | data formatting | bytes 2097152
  8.2 1.0 fusion.28
  9.2 1.2 convolution_convert_fusion.1
  11.1 0.7 convert_element_type.77
  12.2 32.4 %all_gather.13 = bf16[256,128]{1,0:T(8,128)(2,1)S(1)} all-gather(bf16[32,128]{1,0:T(8,128)(2,1)S(1)} %convert_element_type.79), channel_id=1, replica_groups=mesh['sp'=8,'tp'=4] {'sp'}, dimensions={0}, use_global_device_ids=true | all-gather | bytes 73728 | tf_op jit(solution)/shard_map/all_gather | solution.py:106
  44.9 9.4 %all-gather.4.cloned.1.call-done = bf16[256,2048]{1,0:T(8,128)(2,1)} async-done(((bf16[32,2048]{1,0:T(8,128)(2,1)}), bf16[256,2048]{1,0:T(8,128)(2,1)}) %all-gather.4.cloned.1.call-update) | async-done | bytes 1048592 | tf_op jit(solution)/shard_map/all_gather | solution.py:105
  54.3 1.8 %reshape_reshape.3 = bf16[512,4,256]{2,1,0:T(4,128)(2,1)S(1)} reshape(bf16[256,2048]{1,0:T(8,128)(2,1)} %all-gather.4.cloned.1.call-done) | data formatting | bytes 2097152 | tf_op jit(solution)/shard_map/reshape;reshape | solution.py:109
  57.8 1.2 convolution_convert_fusion
  60.0 1.0 scatter_custom_fusion.1
  61.0 1.0 scatter_custom_fusion
  62.1 12.5 %all-gather.6.cloned.1.call-done = bf16[256,2048]{1,0:T(8,128)(2,1)} async-done(((bf16[64,2048]{1,0:T(8,128)(2,1)}), bf16[256,2048]{1,0:T(8,128)(2,1)}) %all-gather.6.cloned.1.call-update) | async-done | bytes 1048592 | tf_op jit(solution)/shard_map/all_gather | solution.py:13
  74.6 1.4 reduce_sum.64
  76.0 1.0 fusion.26
  77.2 1.1 gather_fusion
  78.5 26.1 %all_to_all.10 = bf16[8,24,2048]{2,1,0:T(8,128)(2,1)S(1)} all-to-all(bf16[8,24,2048]{2,1,0:T(8,128)(2,1)S(1)} %broadcast_select_fusion), channel_id=1, replica_groups=mesh['sp'=8,'tp'=4] {'sp'}, dimensions={0} | all-to-all | bytes 1572864 | tf_op jit(solution)/shard_map/all_to_all | solution.py:141
  104.5 3.2 %fusion.4 = f32[192,1024]{1,0:T(8,128)S(1)} fusion(bf16[192,2048]{1,0:T(8,128)(2,1)S(1)} %bitcast.70, bf16[1,2048,1024]{2,1,0:T(8,128)(2,1)} %param.23), kind=kOutput, calls=%fused_computation.8 | convolution fusion | flops 805306368 | bytes 5767168 | tf_op jit(solution)/shard_map/dot_general | solution.py:144
  107.8 1.1 fusion.12
  108.9 1.1 copy-done.6
  109.9 1.9 %fusion.6 = bf16[8,24,2048]{2,1,0:T(8,128)(2,1)} fusion(bf16[8,24,1024]{2,1,0:T(8,128)(2,1)S(1)} %bitcast.75, bf16[1,1024,2048]{2,1,0:T(8,128)(2,1)S(1)} %copy-done.6), kind=kOutput, calls=%fused_computation.10 | convolution fusion | flops 805699584 | bytes 5373952 | tf_op jit(solution)/shard_map/dot_general | solution.py:60
  111.9 21.5 %reduce-scatter.2.cloned.1.call-done = bf16[8,24,512]{2,1,0:T(8,128)(2,1)} async-done(((bf16[8,24,2048]{2,1,0:T(8,128)(2,1)}), bf16[8,24,512]{2,1,0:T(8,128)(2,1)}) %reduce-scatter.2.cloned.1.call-update) | async-done | bytes 196624 | tf_op jit(solution)/shard_map/reduce_scatter | solution.py:63
  133.4 5.5 %all-to-all-start.1 = ((bf16[8,24,512]{2,1,0:T(8,128)(2,1)}), bf16[8,24,512]{2,1,0:T(8,128)(2,1)S(1)}, u32[]{:S(2)}, u32[]{:S(2)}) async-start(bf16[8,24,512]{2,1,0:T(8,128)(2,1)} %reduce-scatter.2.cloned.1.call-done), calls=%async_computation.2 | async-start | bytes 393216 | tf_op jit(solution)/shard_map/all_to_all | solution.py:66
  139.0 7.7 %all-to-all-done.1 = bf16[8,24,512]{2,1,0:T(8,128)(2,1)S(1)} async-done(((bf16[8,24,512]{2,1,0:T(8,128)(2,1)}), bf16[8,24,512]{2,1,0:T(8,128)(2,1)S(1)}, u32[]{:S(2)}, u32[]{:S(2)}) %all-to-all-start.1) | async-done | bytes 196640 | tf_op jit(solution)/shard_map/all_to_all | solution.py:66
  146.7 0.8 gather_fusion.1
  148.1 1.6 %add_convert_fusion.1 = bf16[64,512]{1,0:T(8,128)(2,1)} fusion(f32[64,512]{1,0:T(8,128)S(1)} %multiply_reduce_fusion.1, f32[64,2048]{1,0:T(8,128)} %get-tuple-element.7, s32[]{:T(128)S(6)} %select_n.28), kind=kLoop, calls=%fused_computation.42 | loop fusion | flops 65536 | bytes 327684 | tf_op jit(solution)/shard_map/convert_element_type | solution.py:153
  (61 shorter events, 5.0 us)
Async XLA Ops:
  6.5 51.2 %copy-start = (bf16[512,2048]{1,0:T(8,128)(2,1)S(1)}, bf16[512,2048]{1,0:T(8,128)(2,1)}, u32[]{:S(2)}) copy-start(bf16[512,2048]{1,0:T(8,128)(2,1)} %param.18) | copy-start | bytes 6291460
  6.5 38.2 %slice-start = ((bf16[64,4,192]{2,1,0:T(4,128)(2,1)}), bf16[64,4,64]{2,1,0:T(4,128)(2,1)S(1)}, s32[]{:S(2)}) async-start(bf16[64,4,192]{2,1,0:T(4,128)(2,1)} %param.13), calls=%async_computation.6 | async-start | bytes 131072 | tf_op jit(solution)/shard_map/slice | solution.py:90
  6.5 47.7 %all-gather.4.cloned.1.call-start = ((), (), s32[]{:S(2)}) async-start(), calls=%async_computation.3 | async-start | bytes 1179648 | tf_op jit(solution)/shard_map/all_gather | solution.py:105
  8.1 48.4 %slice-start.1 = ((bf16[64,4,192]{2,1,0:T(4,128)(2,1)}), bf16[64,4,128]{2,1,0:T(4,128)(2,1)S(1)}, s32[]{:S(2)}) async-start(bf16[64,4,192]{2,1,0:T(4,128)(2,1)} %param.13), calls=%async_computation.7 | async-start | bytes 131072 | tf_op jit(solution)/shard_map/slice | solution.py:88
  11.1 63.6 %all-gather.6.cloned.1.call-start = ((), (), s32[]{:S(2)}) async-start(), calls=%async_computation.5 | async-start | bytes 1310720 | tf_op jit(solution)/shard_map/all_gather | solution.py:13
  56.1 2.9 %copy-start.3 = (s32[64,2]{0,1:T(2,128)S(1)}, s32[64,2]{0,1:T(2,128)}, u32[]{:S(2)}) copy-start(s32[64,2]{0,1:T(2,128)} %param.21) | copy-start | bytes 1540
  56.5 19.5 %copy-start.1 = (bf16[64,2048]{1,0:T(8,128)(2,1)S(1)}, bf16[64,2048]{1,0:T(8,128)(2,1)}, u32[]{:S(2)}) copy-start(bf16[64,2048]{1,0:T(8,128)(2,1)} %param.19) | copy-start | bytes 786436
  56.8 20.2 %copy-start.2 = (f32[2048]{0:T(1024)S(1)}, f32[2048]{0:T(1024)}, u32[]{:S(2)}) copy-start(f32[2048]{0:T(1024)} %param.20) | copy-start | bytes 24580
  59.0 74.4 %reduce-scatter.2.cloned.1.call-start = ((), (), s32[]{:S(2)}) async-start(), calls=%async_computation.4 | async-start | bytes 983040 | tf_op jit(solution)/shard_map/reduce_scatter | solution.py:63
  78.3 29.4 %copy-start.5 = (bf16[1,2048,1024]{2,1,0:T(8,128)(2,1)S(1)}, bf16[1,2048,1024]{2,1,0:T(8,128)(2,1)}, u32[]{:S(2)}) copy-start(bf16[1,2048,1024]{2,1,0:T(8,128)(2,1)} %param.24) | copy-start | bytes 12582916
  107.8 2.2 %copy-start.6 = (bf16[1,1024,2048]{2,1,0:T(8,128)(2,1)S(1)}, bf16[1,1024,2048]{2,1,0:T(8,128)(2,1)}, u32[]{:S(2)}) copy-start(bf16[1,1024,2048]{2,1,0:T(8,128)(2,1)} %param.25) | copy-start | bytes 12582916
  108.8 30.0 %copy-start.4 = (f32[64,2]{0,1:T(2,128)S(1)}, f32[64,2]{0,1:T(2,128)}, u32[]{:S(2)}) copy-start(f32[64,2]{0,1:T(2,128)} %param.22) | copy-start | bytes 1540
  133.4 13.3 %all-to-all-start.1 = ((bf16[8,24,512]{2,1,0:T(8,128)(2,1)}), bf16[8,24,512]{2,1,0:T(8,128)(2,1)S(1)}, u32[]{:S(2)}, u32[]{:S(2)}) async-start(bf16[8,24,512]{2,1,0:T(8,128)(2,1)} %reduce-scatter.2.cloned.1.call-done), calls=%async_computation.2 | async-start | bytes 393216 | tf_op jit(solution)/shard_map/all_to_all | solution.py:66
Sparse Core Ops, SparseCore 0:
  11.2 43.0 all-gather.3
  59.1 15.4 all-gather.5
  112.0 21.3 reduce-scatter.1
